TPU v7x, 512 devices: a 4x2x32 block of a 4x8x32 slice. The times are simulated.
512 devices in a mesh: grp: 2 (over y), kv: 64 (over z, core), tp: 4 (over x).
Axes of the slice: x: 4, y: 2, z: 32, core: 2. Of those that a mesh axis runs over, the one named last changes fastest.
The devices are a block of a 4x8x32 slice.
Arguments:
- tokens: bfloat16 [65536, 2048], P(('grp', 'kv')), parts along dimension 0, may hold values from -72 to 72
- w_query: bfloat16 [2048, 1024], P(None, 'tp'), may hold values from -0.125 to 0.125
- w_key: bfloat16 [2048, 256], P(None, 'tp'), may hold values from -0.125 to 0.125
- w_value: bfloat16 [2048, 256], P(None, 'tp'), may hold values from -0.125 to 0.125
- w_out: bfloat16 [1024, 2048], P('tp'), may hold values from -0.1875 to 0.1875
- selection: int32 [4, 1024, 32], P('tp', ('grp', 'kv')), parts along dimension 1, may hold values from -1 to 511, as said below
Outputs:
- attended_out: bfloat16 [65536, 2048], P(('grp', 'kv', 'tp')), parts along dimension 0
There are 2 independent parts, one for each index of `grp`. A program takes and returns all parts, laid end to end along the dimension named above; an argument that names none is the same for every part. Nothing has to cross between parts.
Inputs may be any that keep to these rules, and one draw needn't show every extreme that they name: `selection`: entry 0 is the query block's own index; the others are distinct indices of earlier blocks, then -1 for unused entries. For one key head, the query blocks of one device's range together choose at most 2 distinct blocks of any other device's range, and some device reaches 2 in every draw.
All inputs are finite; a program needn't handle non-finite values.
Results may differ from a plain program's by a relative error of at most 0.028.
The roundings to bfloat16 on the way count: a program that leaves them out, or rounds other values in their place, can miss the bound.
Values may be sent and summed in bfloat16 or wider, within the bound.
No kernel may reach another device: no remote copies, remote signals or barrier semaphores. Data moves between devices by JAX's collectives and lax.ppermute only.
A program may use at most 128 MiB of HBM per device.

v0:
```python
import jax
import jax.numpy as jnp
from jax import lax
from jax.sharding import PartitionSpec as P

HEAD_DIM = 64
BLOCK = 64
TOPK = 32
ROPE_BASE = 500000.0


def cut_along(shard, dim, peers):
    lengths = shard.shape
    tiles = shard.reshape(*lengths[:dim], peers, lengths[dim] // peers, *lengths[dim + 1 :])
    return jnp.moveaxis(tiles, dim, 0)


def sum_at_owner(shard, axis, dim):
    tiles = cut_along(shard, dim, lax.axis_size(axis))
    arrived = lax.all_to_all(tiles, axis, split_axis=0, concat_axis=0, tiled=True)
    return arrived.astype(jnp.float32).sum(axis=0)


def rotate(head_rows, positions):
    half = head_rows.shape[-1] // 2
    freqs = ROPE_BASE ** (-jnp.arange(half, dtype=jnp.float32) / half)
    angles = positions[:, None, None] * freqs
    cosine = jnp.cos(angles)
    sine = jnp.sin(angles)
    first = head_rows[..., :half]
    second = head_rows[..., half:]
    return jnp.concatenate(
        [first * cosine - second * sine, second * cosine + first * sine], axis=-1
    )


def shards(tokens, w_query, w_key, w_value, w_out, selection):
    row_count = tokens.shape[0]
    local_heads = w_query.shape[1] // HEAD_DIM
    own_index = lax.axis_index("kv")
    positions_int = own_index * row_count + jnp.arange(row_count)
    positions = positions_int.astype(jnp.float32)
    queries = rotate(
        jnp.dot(tokens, w_query, preferred_element_type=jnp.float32).reshape(
            row_count, local_heads, HEAD_DIM
        ),
        positions,
    ).astype(jnp.bfloat16)
    key_local = rotate(
        jnp.dot(tokens, w_key, preferred_element_type=jnp.float32).reshape(row_count, 1, HEAD_DIM),
        positions,
    )[:, 0].astype(jnp.bfloat16)
    value_local = jnp.dot(tokens, w_value, preferred_element_type=jnp.float32).astype(jnp.bfloat16)
    key_value = jnp.concatenate([key_local, value_local], axis=-1)
    blocks_here = row_count // BLOCK
    chosen_ids = selection[0]
    key_table = lax.all_gather(key_value, "kv", axis=0, tiled=True).reshape(-1, BLOCK, 2 * HEAD_DIM)
    slot_ids = jnp.maximum(chosen_ids, 0)
    picked = key_table[slot_ids]
    picked_keys = picked[..., :HEAD_DIM].reshape(blocks_here, TOPK * BLOCK, HEAD_DIM)
    picked_values = picked[..., HEAD_DIM:].reshape(blocks_here, TOPK * BLOCK, HEAD_DIM)
    offsets = jnp.arange(BLOCK)
    key_pos = (chosen_ids[:, :, None] * BLOCK + offsets).reshape(blocks_here, TOPK * BLOCK)
    live_keys = jnp.repeat(chosen_ids >= 0, BLOCK, axis=1)
    query_pos = positions_int.reshape(blocks_here, BLOCK)
    query_rows = queries.reshape(blocks_here, BLOCK, local_heads, HEAD_DIM)
    scores = jnp.einsum(
        "qbhd,qkd->qhbk", query_rows, picked_keys, preferred_element_type=jnp.float32
    ) * HEAD_DIM ** (-0.5)
    allowed = live_keys[:, None, None, :] & (
        key_pos[:, None, None, :] <= query_pos[:, None, :, None]
    )
    scores = jnp.where(allowed, scores, -jnp.inf)
    top_score = jnp.max(scores, axis=-1, keepdims=True)
    expo = jnp.exp(scores - top_score)
    weights = (expo / jnp.sum(expo, axis=-1, keepdims=True)).astype(jnp.bfloat16)
    attended = jnp.einsum(
        "qhbk,qkd->qbhd", weights, picked_values, preferred_element_type=jnp.float32
    ).astype(jnp.bfloat16)
    attended = attended.reshape(row_count, local_heads * HEAD_DIM)
    summed = sum_at_owner(
        jnp.dot(attended, w_out, preferred_element_type=jnp.float32).astype(jnp.bfloat16), "tp", 0
    )
    return summed.astype(jnp.bfloat16)


def solution(mesh):
    placed = (
        P(("grp", "kv"), None),
        P(None, "tp"),
        P(None, "tp"),
        P(None, "tp"),
        P("tp", None),
        P("tp", ("grp", "kv"), None),
    )
    return jax.shard_map(
        shards, mesh=mesh, in_specs=placed, out_specs=P(("grp", "kv", "tp"), None), check_vma=False
    )
```

profile of v0, /device:TPU:33, one launch (start us, length us, event | category | flops | bytes accessed | tf_op | source)
XLA Modules:
  0.0 269.1 jit_solution(14196923973627354760)
XLA Ops:
  6.6 1.6 copy-done
  8.1 1.7 convolution_convert_fusion.1
  9.8 1.7 convolution_bitcast_fusion
  11.6 0.3 fusion.16
  11.9 0.7 pad_maximum_fusion.1
  12.6 0.1 all-gather.2.cloned.1.call-update
  12.6 0.0 copy-done.1
  12.7 0.1 reshape.209
  12.7 0.1 add.60
  12.8 0.1 broadcast_in_dim.10
  12.9 0.1 and.16
  13.1 0.1 add.57
  13.2 0.1 add.58
  13.3 0.3 multiply_cosine_fusion
  13.6 2.0 fusion.27
  15.6 0.1 subtract_convert_fusion
  15.6 0.2 concatenate.18
  15.8 1.1 copy.12
  17.0 0.2 concatenate.19
  17.2 1.1 copy.13
  18.3 1.0 compare_and_fusion
  19.3 160.9 %all-gather.2.cloned.1.call-done = bf16[32768,128]{0,1:T(8,128)(2,1)} async-done(((bf16[512,128]{0,1:T(8,128)(2,1)}), bf16[32768,128]{0,1:T(8,128)(2,1)}) %all-gather.2.cloned.1.call-update) | async-done | bytes 8388624 | tf_op jit(solution)/shard_map/all_gather | solution.py:57
  180.2 11.9 %copy.9 = bf16[32768,128]{1,0:T(8,128)(2,1)} copy(bf16[32768,128]{0,1:T(8,128)(2,1)} %all-gather.2.cloned.1.call-done) | data formatting | bytes 16777216 | tf_op jit(solution)/shard_map/all_gather | solution.py:57
  192.1 6.4 %gather_fusion = bf16[256,64,128]{2,1,0:T(8,128)(2,1)} fusion(bf16[512,64,128]{2,1,0:T(8,128)(2,1)} %bitcast.53, s32[1024]{0:T(1024)S(1)} %pad_clamp_fusion), kind=kCustom, calls=%fused_computation | custom fusion | bytes 8389632 | tf_op jit(solution)/shard_map/gather | solution.py:59
  198.5 7.3 %fusion.25 = (bf16[8,32,64,64]{3,2,1,0:T(8,128)(2,1)}, bf16[8,32,64,64]{3,2,1,0:T(8,128)(2,1)}) fusion(bf16[8,32,64,128]{3,2,1,0:T(8,128)(2,1)} %bitcast.52), kind=kLoop, calls=%fused_computation.47 | loop fusion | bytes 8388608 | tf_op jit(solution)/shard_map/slice | solution.py:60
  205.8 10.6 %fusion.26 = (f32[8,4,64]{2,1,0:T(4,128)S(1)}, f32[8,4,64,2048]{3,2,1,0:T(8,128)}) fusion(pred[8,64,2048]{2,1,0:T(8,128)(4,1)S(1)} %compare_and_fusion, bf16[8,2048,64,1]{2,1,3,0:T(8,128)(2,1)} %bitcast.56, bf16[8,64,4,32]{3,1,2,0:T(8,128)(2,1)} %copy.13, bf16[8,64,4,32]{3,1,2,0:T(8,128)(2,1)} %copy.12), kind=kOutput, calls=%fused_computation.48 | convolution fusion | flops 554174464 | bytes 20193280 | tf_op jit(solution)/shard_map/sub | solution.py:75
  216.4 10.7 %fusion.9 = bf16[8,64,4,64]{1,3,2,0:T(8,128)(2,1)S(1)} fusion(bf16[8,2048,64,1]{2,1,3,0:T(8,128)(2,1)} %bitcast.55, f32[8,4,64,2048]{3,2,1,0:T(8,128)} %get-tuple-element.16, f32[8,4,64]{2,1,0:T(4,128)S(1)} %get-tuple-element.15), kind=kOutput, calls=%fused_computation.14 | convolution fusion | flops 545390592 | bytes 19144704 | tf_op jit(solution)/shard_map/qhbk,qkd->qbhd/dot_general | solution.py:77
  227.1 0.3 copy.14
  227.5 0.3 reshape.205
  227.8 2.0 convolution_convert_fusion
  229.8 29.6 %all_to_all.5 = bf16[4,128,2048]{2,1,0:T(8,128)(2,1)} all-to-all(bf16[4,128,2048]{2,1,0:T(8,128)(2,1)S(1)} %bitcast.54), channel_id=1, replica_groups=mesh['grp'=2,'kv'=64,'tp'=4] {'tp'}, dimensions={0} | all-to-all | bytes 4194304 | tf_op jit(solution)/shard_map/all_to_all | solution.py:20
  259.4 2.9 %reduce_sum.22 = bf16[128,2048]{1,0:T(8,128)(2,1)} reduce(bf16[4,128,2048]{2,1,0:T(8,128)(2,1)} %all_to_all.5, bf16[]{:T(256)} %constant.29.clone.1), dimensions={0}, to_apply=%region_2.3 | reduce | flops 786432 | bytes 2621442 | tf_op jit(solution)/shard_map/reduce_sum | solution.py:21
  (12 shorter events, 0.1 us)
Async XLA Ops:
  6.5 1.6 copy-start
  6.6 6.1 %copy-start.1 = (s32[1,8,32]{2,1,0:T(8,128)S(1)}, s32[1,8,32]{2,1,0:T(8,128)}, u32[]{:S(2)}) copy-start(s32[1,8,32]{2,1,0:T(8,128)} %param.11) | copy-start | bytes 3076
  6.6 173.6 %all-gather.2.cloned.1.call-start = ((), (), s32[]{:S(2)}) async-start(), calls=%async_computation.1 | async-start | bytes 8519680 | tf_op jit(solution)/shard_map/all_gather | solution.py:57
Sparse Core Ops, SparseCore 0:
  12.8 167.3 all-gather.1
where the time goes:
time: 270 us; the launch traced here: 269 us
  waiting for transfers between devices  161 us (60%)
  local copies, waits for them, and re-layouts  31 us (11%)
  blocking collectives  29.6 us (11%)
  matrix products  28.6 us (11%)
  between operations  13.6 us (5%)
  other arithmetic  5.32 us (2%)
    all_gather x1, waiting for transfers between devices, shards(): lax.all_gather(key_value, 'kv', axis=0, tiled=True)  161 us
    all_to_all x1, blocking collectives, sum_at_owner(): lax.all_to_all(tiles, axis, split_axis=0, concat_axis=0, tiled=True)  29.6 us
    all_gather x1, local copies, waits for them, and re-layouts, shards(): lax.all_gather(key_value, 'kv', axis=0, tiled=True)  11.9 us
    dot_general x1, matrix products, shards(): jnp.einsum('qhbk,qkd->qbhd', weights, picked_values, preferred_element_ty...  10.7 us
    sub x1, matrix products, shards(): expo = jnp.exp(scores - top_score)  10.6 us
    slice x1, local copies, waits for them, and re-layouts, shards(): picked[..., :HEAD_DIM].reshape(blocks_here, TOPK * BLOCK, HEAD_DIM)  7.28 us
    gather x1, local copies, waits for them, and re-layouts, shards(): picked = key_table[slot_ids]  6.41 us
  transfers between devices with their start and end apart: 1, of which 1 were waited for; matrix products, arithmetic and copies ran while one was open for 2% of the time, Pallas kernels for 0%

commit v1 on v0

--- a/solution.py
+++ b/solution.py
@@ -7,6 +7,11 @@
 BLOCK = 64
 TOPK = 32
 ROPE_BASE = 500000.0
+
+
+def gather_from_all(value, axis, dim):
+    copies = jnp.concatenate([value] * lax.axis_size(axis), axis=dim)
+    return lax.all_to_all(copies, axis, dim, dim, tiled=True)
 
 
 def cut_along(shard, dim, peers):
@@ -54,7 +59,7 @@
     key_value = jnp.concatenate([key_local, value_local], axis=-1)
     blocks_here = row_count // BLOCK
     chosen_ids = selection[0]
-    key_table = lax.all_gather(key_value, "kv", axis=0, tiled=True).reshape(-1, BLOCK, 2 * HEAD_DIM)
+    key_table = gather_from_all(key_value, "kv", 0).reshape(-1, BLOCK, 2 * HEAD_DIM)
     slot_ids = jnp.maximum(chosen_ids, 0)
     picked = key_table[slot_ids]
     picked_keys = picked[..., :HEAD_DIM].reshape(blocks_here, TOPK * BLOCK, HEAD_DIM)

time: 270 us -> 914 us (3.39)
  the two profiles are of different devices: /device:TPU:33 before, /device:TPU:104 now
where the time goes in v1:
time: 914 us
  waiting for transfers between devices  732 us (80%)
  other arithmetic  47.9 us (5%)
  starting transfers between devices  45.4 us (5%)
  blocking collectives  30.7 us (3%)
  local copies, waits for them, and re-layouts  29.7 us (3%)
  matrix products  27.4 us (3%)
    all_to_all x1, waiting for transfers between devices, gather_from_all(): return lax.all_to_all(copies, axis, dim, dim, tiled=True)  732 us
    all_to_all x1, starting transfers between devices, gather_from_all(): return lax.all_to_all(copies, axis, dim, dim, tiled=True)  45.4 us
    unnamed x63, other arithmetic  42.5 us
    all_to_all x1, blocking collectives, sum_at_owner(): lax.all_to_all(tiles, axis, split_axis=0, concat_axis=0, tiled=True)  30.7 us
  transfers between devices with their start and end apart: 1, of which 1 were waited for; matrix products, arithmetic and copies ran while one was open for 0% of the time, Pallas kernels for 0%

profile of v1, /device:TPU:104, one launch (start us, length us, event | category | flops | bytes accessed | tf_op | source)
XLA Modules:
  0.0 913.7 jit_solution(3594036857709022028)
XLA Ops:
  0.0 1.6 copy-done
  1.6 1.7 convolution_convert_fusion.1
  3.3 1.7 convolution_bitcast_fusion
  11.3 0.7 constant_dynamic-update-slice_fusion.54
  12.0 0.7 constant_dynamic-update-slice_fusion.53
  13.4 0.7 constant_dynamic-update-slice_fusion.51
  18.8 0.7 constant_dynamic-update-slice_fusion.43
  20.9 0.7 constant_dynamic-update-slice_fusion.40
  24.2 0.7 constant_dynamic-update-slice_fusion.35
  24.9 0.7 constant_dynamic-update-slice_fusion.34
  26.3 0.7 constant_dynamic-update-slice_fusion.32
  35.0 0.7 constant_dynamic-update-slice_fusion.19
  37.1 0.7 constant_dynamic-update-slice_fusion.16
  37.8 0.7 constant_dynamic-update-slice_fusion.15
  39.1 0.7 constant_dynamic-update-slice_fusion.13
  39.8 0.7 constant_dynamic-update-slice_fusion.12
  45.9 0.7 constant_dynamic-update-slice_fusion.3
  46.6 0.7 constant_dynamic-update-slice_fusion.2
  47.2 0.7 constant_dynamic-update-slice_fusion.1
  47.9 0.7 constant_dynamic-update-slice_fusion
  48.6 11.9 %copy.15 = bf16[32768,128]{1,0:T(8,128)(2,1)} copy(bf16[32768,128]{0,1:T(8,128)(2,1)} %constant_dynamic-update-slice_fusion) | data formatting | bytes 16777216 | tf_op jit(solution)/shard_map/all_to_all | solution.py:14
  60.6 45.4 %all-to-all-start = ((bf16[64,512,128]{2,1,0:T(8,128)(2,1)}), bf16[64,512,128]{2,1,0:T(8,128)(2,1)}, u32[]{:S(2)}, u32[]{:S(2)}) async-start(bf16[64,512,128]{2,1,0:T(8,128)(2,1)} %bitcast.56), calls=%async_computation | async-start | bytes 16777216 | tf_op jit(solution)/shard_map/all_to_all | solution.py:14
  106.9 0.8 fusion.27
  108.9 0.9 compare_and_fusion
  109.8 732.4 %all-to-all-done = bf16[64,512,128]{2,1,0:T(8,128)(2,1)} async-done(((bf16[64,512,128]{2,1,0:T(8,128)(2,1)}), bf16[64,512,128]{2,1,0:T(8,128)(2,1)}, u32[]{:S(2)}, u32[]{:S(2)}) %all-to-all-start) | async-done | bytes 8388640 | tf_op jit(solution)/shard_map/all_to_all | solution.py:14
  842.2 6.4 gather_fusion
  848.6 7.5 fusion.25
  856.2 10.5 %fusion.26 = (f32[8,4,64]{2,1,0:T(4,128)S(1)}, f32[8,4,64,2048]{3,2,1,0:T(8,128)}) fusion(pred[8,64,2048]{2,1,0:T(8,128)(4,1)S(1)} %compare_and_fusion, bf16[8,2048,64,1]{2,1,3,0:T(8,128)(2,1)} %bitcast.59, bf16[8,64,4,32]{3,1,2,0:T(8,128)(2,1)S(1)} %copy.11, bf16[8,64,4,32]{3,1,2,0:T(8,128)(2,1)S(1)} %copy.10), kind=kOutput, calls=%fused_computation.112 | convolution fusion | flops 554174464 | bytes 20193280 | tf_op jit(solution)/shard_map/sub | solution.py:80
  866.7 10.8 %fusion.9 = bf16[8,64,4,64]{1,3,2,0:T(8,128)(2,1)S(1)} fusion(bf16[8,2048,64,1]{2,1,3,0:T(8,128)(2,1)} %bitcast.58, f32[8,4,64,2048]{3,2,1,0:T(8,128)} %get-tuple-element.16, f32[8,4,64]{2,1,0:T(4,128)S(1)} %get-tuple-element.15), kind=kOutput, calls=%fused_computation.14 | convolution fusion | flops 545390592 | bytes 19144704 | tf_op jit(solution)/shard_map/qhbk,qkd->qbhd/dot_general | solution.py:82
  878.2 2.0 convolution_convert_fusion
  880.1 30.7 %all_to_all.14 = bf16[4,128,2048]{2,1,0:T(8,128)(2,1)} all-to-all(bf16[4,128,2048]{2,1,0:T(8,128)(2,1)S(1)} %bitcast.57), channel_id=1, replica_groups=mesh['grp'=2,'kv'=64,'tp'=4] {'tp'}, dimensions={0} | all-to-all | bytes 4194304 | tf_op jit(solution)/shard_map/all_to_all | solution.py:25
  910.8 2.9 reduce_sum.22
  (78 shorter events, 34.5 us)
Async XLA Ops:
  0.0 1.6 copy-start
  60.6 45.4 %copy-start.2 = (s32[1,8,32]{2,1,0:T(8,128)S(1)}, s32[1,8,32]{2,1,0:T(8,128)}, u32[]{:S(2)}) copy-start(s32[1,8,32]{2,1,0:T(8,128)} %param.11) | copy-start | bytes 3076
  60.6 46.4 %copy-start.3 = (bf16[2048,256]{1,0:T(8,128)(2,1)S(1)}, bf16[2048,256]{1,0:T(8,128)(2,1)}, u32[]{:S(2)}) copy-start(bf16[2048,256]{1,0:T(8,128)(2,1)} %param.7) | copy-start | bytes 3145732
  60.6 781.6 %all-to-all-start = ((bf16[64,512,128]{2,1,0:T(8,128)(2,1)}), bf16[64,512,128]{2,1,0:T(8,128)(2,1)}, u32[]{:S(2)}, u32[]{:S(2)}) async-start(bf16[64,512,128]{2,1,0:T(8,128)(2,1)} %bitcast.56), calls=%async_computation | async-start | bytes 16777216 | tf_op jit(solution)/shard_map/all_to_all | solution.py:14
  866.7 47.1 %copy-start.1 = (bf16[512,2048]{1,0:T(8,128)(2,1)S(1)}, bf16[512,2048]{1,0:T(8,128)(2,1)}, u32[]{:S(2)}) copy-start(bf16[512,2048]{1,0:T(8,128)(2,1)} %param.6) | copy-start | bytes 6291460
